TPU v7x, 32 devices: a whole 2x2x4 slice. The times are simulated.
32 devices in a mesh: ep: 8 (over z, y), tp: 4 (over x, core).
Axes of the slice: x: 2, y: 2, z: 4, core: 2. Of those that a mesh axis runs over, the one named last changes fastest.
Arguments:
- tokens: bfloat16 [6144, 2048], P('ep')
- in_gain: float32 [2048], replicated, may hold values from 0.1 to 1.9
- route_ids: int32 [6144, 2], P('ep'), may hold values from 0 to 7, all different within a row; in each aligned block of 768 rows (0 to 767, 768 to 1535, ...) at most 384 rows name the same one
- route_scores: float32 [6144, 2], P('ep'), may hold values from 0.1 to 1
- gate_weight: bfloat16 [8, 2048, 1024], P('ep', None, 'tp'), may hold values from -0.125 to 0.125
- up_weight: bfloat16 [8, 2048, 1024], P('ep', None, 'tp'), may hold values from -0.125 to 0.125
- down_weight: bfloat16 [8, 1024, 2048], P('ep', 'tp')
- out_gain: float32 [2048], P('tp'), may hold values from 0.1 to 1.9
Outputs:
- mixed: bfloat16 [6144, 2048], P('ep', 'tp')
Inputs may be any that keep to these rules, and one draw needn't show every extreme that they name: `route_ids`: each row names 2 different experts. Among the rows of one index of ep (aligned blocks of 768 rows) no expert is named more than 384 times, a bound that some block reaches.
All inputs are finite; a program needn't handle non-finite values.
Results may differ from a plain program's by a relative error of at most 0.012.
Values may be sent and summed in bfloat16 or wider, within the bound.
A program may use at most 128 MiB of HBM per device.

v0:
```python
import jax
import jax.numpy as jnp
from jax import lax
from jax.sharding import PartitionSpec as P

epsilon = 1e-06


def per_device(
    tokens, in_gain, route_ids, route_scores, gate_weight, up_weight, down_weight, out_gain
):
    count_ep = lax.axis_size("ep")
    count_tp = lax.axis_size("tp")
    local_experts = gate_weight.shape[0]
    experts = count_ep * local_experts
    tok_count, full_width = tokens.shape
    choose_count = route_ids.shape[1]
    capacity = 2 * tok_count * choose_count // experts
    part_width = full_width // count_tp
    as_float = tokens.astype(jnp.float32)
    normed = (
        as_float
        * lax.rsqrt(jnp.mean(as_float * as_float, axis=1, keepdims=True) + epsilon)
        * in_gain
    ).astype(jnp.bfloat16)
    flat_ids = route_ids.reshape(-1)
    one_hot = (flat_ids[:, None] == jnp.arange(experts, dtype=jnp.int32)[None, :]).astype(jnp.int32)
    slot_index = jnp.sum((jnp.cumsum(one_hot, axis=0) - 1) * one_hot, axis=1)
    row_index = jnp.arange(tok_count * choose_count, dtype=jnp.int32) // choose_count
    own_slice = lax.dynamic_slice_in_dim(normed, lax.axis_index("tp") * part_width, part_width, 1)
    buffer = jnp.zeros((experts, capacity, part_width), jnp.bfloat16)
    buffer = buffer.at[flat_ids, slot_index].set(own_slice[row_index])
    buffer = buffer.reshape(count_ep, local_experts, capacity, part_width)
    received = lax.all_to_all(buffer, "ep", split_axis=0, concat_axis=0, tiled=True)
    piece = lax.all_gather(received, "tp", axis=3, tiled=True)
    gate_add = jnp.einsum("secn,enf->secf", piece, gate_weight, preferred_element_type=jnp.float32)
    up_add = jnp.einsum("secn,enf->secf", piece, up_weight, preferred_element_type=jnp.float32)
    hidden = (jax.nn.silu(gate_add) * up_add).astype(jnp.bfloat16)
    partial_terms = jnp.einsum(
        "secf,efd->secd", hidden, down_weight, preferred_element_type=jnp.float32
    ).astype(jnp.bfloat16)
    summed = (
        lax.psum_scatter(partial_terms, "tp", scatter_dimension=3, tiled=True)
        .astype(jnp.float32)
        .astype(jnp.bfloat16)
    )
    returned = lax.all_to_all(summed, "ep", split_axis=0, concat_axis=0, tiled=True).reshape(
        experts, capacity, part_width
    )
    picked = (
        returned[flat_ids, slot_index]
        .astype(jnp.float32)
        .reshape(tok_count, choose_count, part_width)
    )
    mix_weight = route_scores / jnp.sum(route_scores, axis=1, keepdims=True)
    combined = jnp.sum(mix_weight[:, :, None] * picked, axis=1)
    squares_sum = lax.psum(jnp.sum(combined * combined, axis=1), "tp")
    scaled = combined * lax.rsqrt(squares_sum[:, None] / full_width + epsilon) * out_gain
    return scaled.astype(jnp.bfloat16)


def solution(mesh):
    in_specs = (
        P("ep", None),
        P(),
        P("ep", None),
        P("ep", None),
        P("ep", None, "tp"),
        P("ep", None, "tp"),
        P("ep", "tp", None),
        P("tp"),
    )
    out_specs = P("ep", "tp")
    return jax.shard_map(
        per_device, mesh=mesh, in_specs=in_specs, out_specs=out_specs, check_vma=False
    )
```

profile of v0, /device:TPU:0, one launch (start us, length us, event | category | flops | bytes accessed | tf_op | source)
XLA Modules:
  0.0 441.9 jit_solution(14998475770619304312)
XLA Ops:
  6.5 1.0 copy.15
  7.5 0.2 eq.29
  7.7 0.2 eq.25
  8.0 0.2 reshape.152
  8.2 5.5 %convert_element_type.39 = f32[768,2048]{1,0:T(8,128)} convert(bf16[768,2048]{1,0:T(8,128)(2,1)} %param.8) | non-fusion elementwise | flops 1572864 | bytes 9437184 | tf_op jit(solution)/shard_map/convert_element_type | solution.py:20
  13.8 0.7 multiply_reduce_fusion
  14.5 0.1 fusion.27
  14.5 2.3 reduce-window.6
  16.8 0.3 slice_reduce_fusion
  17.1 0.2 reduce-window.9
  17.3 0.1 add_bitcast_fusion
  17.5 0.1 multiply_reduce_fusion.3
  17.6 0.1 and_reduce_fusion
  17.7 0.8 dynamic-slice
  18.5 1.6 fusion.11
  20.1 16.3 %scatter_custom_fusion = bf16[3072,512]{1,0:T(8,128)(2,1)} fusion(s32[1536]{0:T(1024)S(1)} %broadcast_select_fusion, bf16[768,512]{1,0:T(8,128)(2,1)S(1)} %fusion.11, s32[2048]{0:T(1024)S(1)} %pad_clamp_fusion, bf16[]{:T(256)} %constant.38.clone.1), kind=kCustom, calls=%fused_computation.21 | custom fusion | bytes 3145730
  36.4 78.1 %all_to_all.10 = bf16[8,1,384,512]{3,2,1,0:T(8,128)(2,1)} all-to-all(bf16[8,1,384,512]{3,2,1,0:T(8,128)(2,1)} %bitcast.86), channel_id=1, replica_groups=mesh['ep'=8,'tp'=4] {'ep'}, dimensions={0} | all-to-all | bytes 6291456 | tf_op jit(solution)/shard_map/all_to_all | solution.py:34
  114.5 0.0 all-gather.2.cloned.1.call-update
  114.6 0.2 reduce-scatter.2.cloned.1.call-start
  114.8 81.0 %all-gather.2.cloned.1.call-done = bf16[8,1,384,2048]{3,2,0,1:T(8,128)(2,1)} async-done(((bf16[8,1,384,512]{3,2,0,1:T(8,128)(2,1)}), bf16[8,1,384,2048]{3,2,0,1:T(8,128)(2,1)}) %all-gather.2.cloned.1.call-update) | async-done | bytes 12582928 | tf_op jit(solution)/shard_map/all_gather | solution.py:35
  195.8 9.8 %fusion.2 = f32[8,384,256]{2,1,0:T(8,128)} fusion(bf16[8,1,384,2048]{3,2,0,1:T(8,128)(2,1)} %all-gather.2.cloned.1.call-done, bf16[1,2048,256]{2,1,0:T(8,128)(2,1)S(1)} %copy-done.6), kind=kOutput, calls=%fused_computation.5 | convolution fusion | flops 3221225472 | bytes 16777216 | tf_op jit(solution)/shard_map/secn,enf->secf/dot_general | solution.py:36
  205.6 18.8 %convert_bitcast_fusion = bf16[8,1,384,2048]{3,2,0,1:T(8,128)(2,1)} fusion(f32[8,384,256]{2,1,0:T(8,128)} %fusion.2, bf16[8,1,384,2048]{3,2,0,1:T(8,128)(2,1)} %all-gather.2.cloned.1.call-done, bf16[1,256,2048]{2,1,0:T(8,128)(2,1)S(1)} %copy-done, bf16[1,2048,256]{2,1,0:T(8,128)(2,1)S(1)} %copy-done.7), kind=kOutput, calls=%fused_computation.7 | convolution fusion | flops 6453460992 | bytes 30408704 | tf_op jit(solution)/shard_map/secf,efd->secd/dot_general | solution.py:39
  224.4 97.3 %reduce-scatter.2.cloned.1.call-done = bf16[8,1,384,512]{3,2,0,1:T(8,128)(2,1)} async-done(((bf16[8,1,384,2048]{3,2,0,1:T(8,128)(2,1)}), bf16[8,1,384,512]{3,2,0,1:T(8,128)(2,1)}) %reduce-scatter.2.cloned.1.call-update) | async-done | bytes 3145744 | tf_op jit(solution)/shard_map/reduce_scatter | solution.py:43
  321.7 5.6 %all-to-all-start.1 = ((bf16[8,1,384,512]{3,2,1,0:T(8,128)(2,1)}), bf16[8,1,384,512]{3,2,1,0:T(8,128)(2,1)}, u32[]{:S(2)}, u32[]{:S(2)}) async-start(bf16[8,1,384,512]{3,2,1,0:T(8,128)(2,1)} %bitcast.87), calls=%async_computation.2 | async-start | bytes 6291456 | tf_op jit(solution)/shard_map/all_to_all | solution.py:47
  327.4 0.2 copy.14
  327.6 70.4 %all-to-all-done.1 = bf16[8,1,384,512]{3,2,1,0:T(8,128)(2,1)} async-done(((bf16[8,1,384,512]{3,2,1,0:T(8,128)(2,1)}), bf16[8,1,384,512]{3,2,1,0:T(8,128)(2,1)}, u32[]{:S(2)}, u32[]{:S(2)}) %all-to-all-start.1) | async-done | bytes 3145760 | tf_op jit(solution)/shard_map/all_to_all | solution.py:47
  398.0 20.5 %gather_fusion = bf16[1536,512]{1,0:T(8,128)(2,1)S(1)} fusion(bf16[8,384,512]{2,1,0:T(8,128)(2,1)} %bitcast.23, s32[1536]{0:T(1024)S(1)} %get-tuple-element.5), kind=kCustom, calls=%fused_computation.1 | custom fusion | bytes 3158016 | tf_op jit(solution)/shard_map/gather | solution.py:51
  418.5 3.3 reshape.166
  421.8 6.0 %multiply_reduce_fusion.1 = f32[768,512]{1,0:T(8,128)S(1)} fusion(f32[768,2,512]{2,1,0:T(2,128)} %reshape.166, f32[768,2]{1,0:T(8,128)S(1)} %copy.14), kind=kLoop, calls=%fused_computation.16 | loop fusion | flops 1179648 | bytes 4724736 | tf_op jit(solution)/shard_map/reduce_sum | solution.py:56
  427.8 0.2 multiply_reduce_fusion.2
  428.0 6.0 %psum.7 = f32[768]{0:T(1024)S(1)} all-reduce(f32[768]{0:T(1024)S(1)} %multiply_reduce_fusion.2), channel_id=1, replica_groups=mesh['ep'=8,'tp'=4] {'tp'}, use_global_device_ids=true, to_apply=%region_9.10 | all-reduce | flops 768 | bytes 6144 | tf_op jit(solution)/shard_map/psum | solution.py:57
  434.0 1.1 multiply_convert_fusion
  (27 shorter events, 0.2 us)
Async XLA Ops:
  6.5 199.1 %copy-start = (bf16[1,256,2048]{2,1,0:T(8,128)(2,1)S(1)}, bf16[1,256,2048]{2,1,0:T(8,128)(2,1)}, u32[]{:S(2)}) copy-start(bf16[1,256,2048]{2,1,0:T(8,128)(2,1)} %param.14) | copy-start | bytes 3145732
  6.5 189.3 %all-gather.2.cloned.1.call-start = ((), (), s32[]{:S(2)}) async-start(), calls=%async_computation.3 | async-start | bytes 15728640 | tf_op jit(solution)/shard_map/all_gather | solution.py:35
  8.2 5.6 %copy-start.1 = (bf16[768,2048]{1,0:T(8,128)(2,1)S(1)}, bf16[768,2048]{1,0:T(8,128)(2,1)}, u32[]{:S(2)}) copy-start(bf16[768,2048]{1,0:T(8,128)(2,1)} %param.8) | copy-start | bytes 9437188
  13.8 3.7 copy-start.5
  13.8 3.8 copy-start.4
  114.5 81.3 %copy-start.6 = (bf16[1,2048,256]{2,1,0:T(8,128)(2,1)S(1)}, bf16[1,2048,256]{2,1,0:T(8,128)(2,1)}, u32[]{:S(2)}) copy-start(bf16[1,2048,256]{2,1,0:T(8,128)(2,1)} %param.12) | copy-start | bytes 3145732
  114.6 91.0 %copy-start.7 = (bf16[1,2048,256]{2,1,0:T(8,128)(2,1)S(1)}, bf16[1,2048,256]{2,1,0:T(8,128)(2,1)}, u32[]{:S(2)}) copy-start(bf16[1,2048,256]{2,1,0:T(8,128)(2,1)} %param.13) | copy-start | bytes 3145732
  114.6 207.2 %reduce-scatter.2.cloned.1.call-start = ((), (), s32[]{:S(2)}) async-start(), calls=%async_computation.4 | async-start | bytes 15728640 | tf_op jit(solution)/shard_map/reduce_scatter | solution.py:43
  321.7 5.6 %copy-start.2 = (f32[768,2]{0,1:T(2,128)S(1)}, f32[768,2]{0,1:T(2,128)}, u32[]{:S(2)}) copy-start(f32[768,2]{0,1:T(2,128)} %param.11) | copy-start | bytes 18436
  321.7 76.3 %all-to-all-start.1 = ((bf16[8,1,384,512]{3,2,1,0:T(8,128)(2,1)}), bf16[8,1,384,512]{3,2,1,0:T(8,128)(2,1)}, u32[]{:S(2)}, u32[]{:S(2)}) async-start(bf16[8,1,384,512]{3,2,1,0:T(8,128)(2,1)} %bitcast.87), calls=%async_computation.2 | async-start | bytes 6291456 | tf_op jit(solution)/shard_map/all_to_all | solution.py:47
  421.8 12.2 %copy-start.3 = (f32[512]{0:T(512)S(1)}, f32[512]{0:T(512)}, u32[]{:S(2)}) copy-start(f32[512]{0:T(512)} %param.15) | copy-start | bytes 6148
Sparse Core Ops, SparseCore 0:
  114.7 81.0 all-gather.1
  224.5 97.1 reduce-scatter.1
where the time goes:
time: 443 us; the launch traced here: 442 us
  waiting for transfers between devices  249 us (56%)
  blocking collectives  84.1 us (19%)
  local copies, waits for them, and re-layouts  43 us (10%)
  matrix products  28.6 us (6%)
  other arithmetic  18 us (4%)
  between operations  13.6 us (3%)
  starting transfers between devices  5.85 us (1%)
    reduce_scatter x1, waiting for transfers between devices, per_device(): lax.psum_scatter(partial_terms, 'tp', scatter_dimension=3, tiled=True)  97.3 us
    all_gather x1, waiting for transfers between devices, per_device(): piece = lax.all_gather(received, 'tp', axis=3, tiled=True)  81 us
    all_to_all x1, blocking collectives, per_device(): lax.all_to_all(buffer, 'ep', split_axis=0, concat_axis=0, tiled=True)  78.1 us
    all_to_all x1, waiting for transfers between devices, per_device(): lax.all_to_all(summed, 'ep', split_axis=0, concat_axis=0, tiled=True)  70.4 us
    gather x1, local copies, waits for them, and re-layouts, per_device(): returned[flat_ids, slot_index].astype(jnp.float32)  20.5 us
    dot_general x1, matrix products, per_device(): jnp.einsum('secf,efd->secd', hidden, down_weight, preferred_element_type=...  18.8 us
    unnamed x18, local copies, waits for them, and re-layouts  17.3 us
    dot_general x1, matrix products, per_device(): jnp.einsum('secn,enf->secf', piece, gate_weight, preferred_element_type=j...  9.79 us
  transfers between devices with their start and end apart: 3, of which 3 were waited for; matrix products, arithmetic and copies ran while one was open for 0% of the time, Pallas kernels for 0%

commit v1 on v0

--- a/solution.py
+++ b/solution.py
@@ -32,7 +32,8 @@
     buffer = buffer.at[flat_ids, slot_index].set(own_slice[row_index])
     buffer = buffer.reshape(count_ep, local_experts, capacity, part_width)
     received = lax.all_to_all(buffer, "ep", split_axis=0, concat_axis=0, tiled=True)
-    piece = lax.all_gather(received, "tp", axis=3, tiled=True)
+    parts = lax.all_gather(received, "tp")
+    piece = jnp.concatenate(parts, axis=3)
     gate_add = jnp.einsum("secn,enf->secf", piece, gate_weight, preferred_element_type=jnp.float32)
     up_add = jnp.einsum("secn,enf->secf", piece, up_weight, preferred_element_type=jnp.float32)
     hidden = (jax.nn.silu(gate_add) * up_add).astype(jnp.bfloat16)

time: 443 us -> 479 us (1.081)
  local copies, waits for them, and re-layouts: 43 us -> 78.7 us
    another operation x0 -> x1, local copies, waits for them, and re-layouts: none -> 21 us
    reshape x0 -> x1, local copies, waits for them, and re-layouts: none -> 15.6 us  [per_device(): piece = jnp.concatenate(parts, axis=3)]
    unnamed x18 -> x20, local copies, waits for them, and re-layouts: 17.3 us -> 17.3 us
where the time goes in v1:
time: 479 us; the launch traced here: 478 us
  waiting for transfers between devices  249 us (52%)
  blocking collectives  84.1 us (18%)
  local copies, waits for them, and re-layouts  78.7 us (16%)
  matrix products  28.7 us (6%)
  other arithmetic  18.1 us (4%)
  between operations  13.6 us (3%)
  starting transfers between devices  5.87 us (1%)
    reduce_scatter x1, waiting for transfers between devices, per_device(): lax.psum_scatter(partial_terms, 'tp', scatter_dimension=3, tiled=True)  97.3 us
    all_gather x1, waiting for transfers between devices, per_device(): parts = lax.all_gather(received, 'tp')  81 us
    all_to_all x1, blocking collectives, per_device(): lax.all_to_all(buffer, 'ep', split_axis=0, concat_axis=0, tiled=True)  78.1 us
    all_to_all x1, waiting for transfers between devices, per_device(): lax.all_to_all(summed, 'ep', split_axis=0, concat_axis=0, tiled=True)  70.3 us
    another operation x1, local copies, waits for them, and re-layouts  21 us
    dot_general x1, matrix products, per_device(): jnp.einsum('secf,efd->secd', hidden, down_weight, preferred_element_type=...  18.8 us
    gather x1, local copies, waits for them, and re-layouts, per_device(): returned[flat_ids, slot_index].astype(jnp.float32)  18 us
    unnamed x20, local copies, waits for them, and re-layouts  17.3 us
  transfers between devices with their start and end apart: 3, of which 3 were waited for; matrix products, arithmetic and copies ran while one was open for 0% of the time, Pallas kernels for 0%

profile of v1, /device:TPU:0, one launch (start us, length us, event | category | flops | bytes accessed | tf_op | source)
XLA Modules:
  0.0 477.6 jit_solution(2302486951629735300)
XLA Ops:
  6.5 1.0 copy.16
  7.5 0.2 eq.29
  7.7 0.2 eq.25
  8.0 0.2 reshape.158
  8.2 5.5 %convert_element_type.39 = f32[768,2048]{1,0:T(8,128)} convert(bf16[768,2048]{1,0:T(8,128)(2,1)} %param.8) | non-fusion elementwise | flops 1572864 | bytes 9437184 | tf_op jit(solution)/shard_map/convert_element_type | solution.py:20
  13.8 0.7 multiply_reduce_fusion
  14.5 2.3 reduce-window.6
  16.8 0.3 slice_reduce_fusion
  17.1 0.2 reduce-window.9
  17.3 0.1 add_bitcast_fusion
  17.5 0.1 multiply_reduce_fusion.3
  17.6 0.1 and_reduce_fusion
  17.7 0.8 dynamic-slice
  18.5 1.6 fusion.5
  20.1 16.3 %scatter_custom_fusion = bf16[3072,512]{1,0:T(8,128)(2,1)} fusion(s32[1536]{0:T(1024)S(1)} %broadcast_select_fusion, bf16[768,512]{1,0:T(8,128)(2,1)S(1)} %fusion.5, s32[2048]{0:T(1024)S(1)} %pad_clamp_fusion, bf16[]{:T(256)} %constant.38.clone.1), kind=kCustom, calls=%fused_computation.17 | custom fusion | bytes 3145730
  36.4 78.1 %all_to_all.10 = bf16[8,1,384,512]{3,2,1,0:T(8,128)(2,1)} all-to-all(bf16[8,1,384,512]{3,2,1,0:T(8,128)(2,1)} %bitcast.85), channel_id=1, replica_groups=mesh['ep'=8,'tp'=4] {'ep'}, dimensions={0} | all-to-all | bytes 6291456 | tf_op jit(solution)/shard_map/all_to_all | solution.py:34
  114.6 0.2 reduce-scatter.2.cloned.1.call-start
  114.8 81.0 %all-gather.3.cloned.1.call-done = bf16[32,1,384,512]{3,2,1,0:T(8,128)(2,1)} async-done(((bf16[8,1,384,512]{3,2,1,0:T(8,128)(2,1)}), bf16[32,1,384,512]{3,2,1,0:T(8,128)(2,1)}) %all-gather.3.cloned.1.call-update) | async-done | bytes 12582928 | tf_op jit(solution)/shard_map/all_gather | solution.py:35
  195.8 15.6 %copy.19 = bf16[8,1,384,4,512]{4,3,2,0,1:T(4,128)(2,1)} copy(bf16[8,1,384,4,512]{4,2,0,3,1:T(8,128)(2,1)} %bitcast.84) | data formatting | bytes 25165824 | tf_op jit(solution)/shard_map/reshape | solution.py:36
  211.4 21.0 %reshape.162 = bf16[8,384,2048]{2,1,0:T(8,128)(2,1)} reshape(bf16[8,1,384,4,512]{4,3,2,0,1:T(4,128)(2,1)} %copy.19) | data formatting | bytes 25165824 | tf_op jit(solution)/shard_map/reshape.4
  232.4 9.9 %fusion.11 = f32[8,384,256]{2,1,0:T(8,128)} fusion(bf16[8,384,2048]{2,1,0:T(8,128)(2,1)} %reshape.162, bf16[1,2048,256]{2,1,0:T(8,128)(2,1)S(1)} %copy-done.7), kind=kOutput, calls=%fused_computation.23 | convolution fusion | flops 3221225472 | bytes 16777216 | tf_op jit(solution)/shard_map/secn,enf->secf/dot_general | solution.py:38
  242.3 18.8 %convert_bitcast_fusion = bf16[8,1,384,2048]{3,2,0,1:T(8,128)(2,1)} fusion(bf16[1,256,2048]{2,1,0:T(8,128)(2,1)S(1)} %copy-done, f32[8,384,256]{2,1,0:T(8,128)} %fusion.11, bf16[8,384,2048]{2,1,0:T(8,128)(2,1)} %reshape.162, bf16[1,2048,256]{2,1,0:T(8,128)(2,1)S(1)} %copy-done.8), kind=kOutput, calls=%fused_computation.3 | convolution fusion | flops 6453460992 | bytes 30408704 | tf_op jit(solution)/shard_map/secf,efd->secd/dot_general | solution.py:40
  261.2 97.3 %reduce-scatter.2.cloned.1.call-done = bf16[8,1,384,512]{3,2,0,1:T(8,128)(2,1)} async-done(((bf16[8,1,384,2048]{3,2,0,1:T(8,128)(2,1)}), bf16[8,1,384,512]{3,2,0,1:T(8,128)(2,1)}) %reduce-scatter.2.cloned.1.call-update) | async-done | bytes 3145744 | tf_op jit(solution)/shard_map/reduce_scatter | solution.py:44
  358.4 5.6 %all-to-all-start.1 = ((bf16[8,1,384,512]{3,2,1,0:T(8,128)(2,1)}), bf16[8,1,384,512]{3,2,1,0:T(8,128)(2,1)S(1)}, u32[]{:S(2)}, u32[]{:S(2)}) async-start(bf16[8,1,384,512]{3,2,1,0:T(8,128)(2,1)} %bitcast.86), calls=%async_computation.2 | async-start | bytes 6291456 | tf_op jit(solution)/shard_map/all_to_all | solution.py:48
  364.1 0.2 copy.15
  364.3 70.3 %all-to-all-done.1 = bf16[8,1,384,512]{3,2,1,0:T(8,128)(2,1)S(1)} async-done(((bf16[8,1,384,512]{3,2,1,0:T(8,128)(2,1)}), bf16[8,1,384,512]{3,2,1,0:T(8,128)(2,1)S(1)}, u32[]{:S(2)}, u32[]{:S(2)}) %all-to-all-start.1) | async-done | bytes 3145760 | tf_op jit(solution)/shard_map/all_to_all | solution.py:48
  434.7 18.0 %gather_fusion = bf16[1536,512]{1,0:T(8,128)(2,1)} fusion(bf16[8,384,512]{2,1,0:T(8,128)(2,1)S(1)} %bitcast.83, s32[1536]{0:T(1024)S(1)} %get-tuple-element.5), kind=kCustom, calls=%fused_computation.1 | custom fusion | bytes 3158016 | tf_op jit(solution)/shard_map/gather | solution.py:52
  452.7 4.7 reshape.173
  457.4 6.1 %multiply_reduce_fusion.1 = f32[768,512]{1,0:T(8,128)S(1)} fusion(f32[768,2,512]{2,1,0:T(2,128)} %reshape.173, f32[768,2]{1,0:T(8,128)S(1)} %copy.15), kind=kLoop, calls=%fused_computation.12 | loop fusion | flops 1179648 | bytes 4724736 | tf_op jit(solution)/shard_map/reduce_sum | solution.py:57
  463.5 0.2 multiply_reduce_fusion.2
  463.7 6.0 %psum.7 = f32[768]{0:T(1024)S(1)} all-reduce(f32[768]{0:T(1024)S(1)} %multiply_reduce_fusion.2), channel_id=1, replica_groups=mesh['ep'=8,'tp'=4] {'tp'}, use_global_device_ids=true, to_apply=%region_9.10 | all-reduce | flops 768 | bytes 6144 | tf_op jit(solution)/shard_map/psum | solution.py:58
  469.7 1.1 multiply_convert_fusion
  (31 shorter events, 0.3 us)
Async XLA Ops:
  6.5 235.8 %copy-start = (bf16[1,256,2048]{2,1,0:T(8,128)(2,1)S(1)}, bf16[1,256,2048]{2,1,0:T(8,128)(2,1)}, u32[]{:S(2)}) copy-start(bf16[1,256,2048]{2,1,0:T(8,128)(2,1)} %param.14) | copy-start | bytes 3145732
  6.5 189.3 %all-gather.3.cloned.1.call-start = ((), (), s32[]{:S(2)}) async-start(), calls=%async_computation.4 | async-start | bytes 15728640 | tf_op jit(solution)/shard_map/all_gather | solution.py:35
  8.2 5.6 %copy-start.2 = (bf16[768,2048]{1,0:T(8,128)(2,1)S(1)}, bf16[768,2048]{1,0:T(8,128)(2,1)}, u32[]{:S(2)}) copy-start(bf16[768,2048]{1,0:T(8,128)(2,1)} %param.8) | copy-start | bytes 9437188
  13.8 3.7 copy-start.6
  13.8 3.8 copy-start.5
  114.6 243.9 %reduce-scatter.2.cloned.1.call-start = ((), (), s32[]{:S(2)}) async-start(), calls=%async_computation.3 | async-start | bytes 15728640 | tf_op jit(solution)/shard_map/reduce_scatter | solution.py:44
  211.4 21.0 %copy-start.7 = (bf16[1,2048,256]{2,1,0:T(8,128)(2,1)S(1)}, bf16[1,2048,256]{2,1,0:T(8,128)(2,1)}, u32[]{:S(2)}) copy-start(bf16[1,2048,256]{2,1,0:T(8,128)(2,1)} %param.13) | copy-start | bytes 3145732
  232.4 9.9 %copy-start.8 = (bf16[1,2048,256]{2,1,0:T(8,128)(2,1)S(1)}, bf16[1,2048,256]{2,1,0:T(8,128)(2,1)}, u32[]{:S(2)}) copy-start(bf16[1,2048,256]{2,1,0:T(8,128)(2,1)} %param.12) | copy-start | bytes 3145732
  358.4 5.7 %copy-start.3 = (f32[768,2]{0,1:T(2,128)S(1)}, f32[768,2]{0,1:T(2,128)}, u32[]{:S(2)}) copy-start(f32[768,2]{0,1:T(2,128)} %param.11) | copy-start | bytes 18436
  358.4 76.2 %all-to-all-start.1 = ((bf16[8,1,384,512]{3,2,1,0:T(8,128)(2,1)}), bf16[8,1,384,512]{3,2,1,0:T(8,128)(2,1)S(1)}, u32[]{:S(2)}, u32[]{:S(2)}) async-start(bf16[8,1,384,512]{3,2,1,0:T(8,128)(2,1)} %bitcast.86), calls=%async_computation.2 | async-start | bytes 6291456 | tf_op jit(solution)/shard_map/all_to_all | solution.py:48
  457.4 12.2 %copy-start.4 = (f32[512]{0:T(512)S(1)}, f32[512]{0:T(512)}, u32[]{:S(2)}) copy-start(f32[512]{0:T(512)} %param.15) | copy-start | bytes 6148
  457.4 13.3 %copy-start.1 = (bf16[1,256,2048]{2,1,0:T(8,128)(2,1)S(1)}, bf16[1,256,2048]{2,1,0:T(8,128)(2,1)}, u32[]{:S(2)}) copy-start(bf16[1,256,2048]{2,1,0:T(8,128)(2,1)} %param.14) | copy-start | bytes 3145732
Sparse Core Ops, SparseCore 0:
  114.7 81.0 all-gather.2
  261.3 97.1 reduce-scatter.1
